TPU v7x, 512 devices: a whole 4x4x16 slice. The times are simulated.
512 devices in a mesh: ep: 32 (over z, core), tp: 16 (over y, x).
Axes of the slice: x: 4, y: 4, z: 16, core: 2. Of those that a mesh axis runs over, the one named last changes fastest.
Arguments:
- query_rows: bfloat16 [16384, 2048], P('ep', 'tp'), may hold values from -6 to 6
- key_rows: bfloat16 [16384, 2048], P('ep', 'tp'), may hold values from -6 to 6
- value_rows: bfloat16 [16384, 4096], P('ep', 'tp'), may hold values from -6 to 6
- in_gate: float32 [16, 16384], P('tp', 'ep'), may hold values from -120 to 120
- forget_gate: float32 [16, 16384], P('tp', 'ep'), may hold values from -2 to 20
- out_gate: bfloat16 [16384, 4096], P('ep', 'tp'), may hold values from -6 to 6
- head_gain: float32 [4096], P('tp'), may hold values from 0.1 to 1.9
- mix_weight: bfloat16 [4096, 4096], P(None, 'tp'), may hold values from -0.09375 to 0.09375
- expert_input: bfloat16 [8192, 4096], P('ep', 'tp'), may hold values from -30 to 30
- routes: int32 [8192, 2], P('ep'), may hold values from 0 to 31, all different within a row; in each aligned block of 256 rows (0 to 255, 256 to 511, ...) at most 32 rows name the same one
- route_weight: float32 [8192, 2], P('ep'), may hold values from 0.25 to 1.25
- gate_weight: bfloat16 [32, 1024, 4096], P('ep', 'tp'), may hold values from -0.09375 to 0.09375
- up_weight: bfloat16 [32, 1024, 4096], P('ep', 'tp'), may hold values from -0.09375 to 0.09375
- down_weight: bfloat16 [32, 1024, 4096], P('ep', None, 'tp'), may hold values from -0.1875 to 0.1875
Outputs:
- mixer_out: bfloat16 [16384, 4096], P('ep', 'tp')
- expert_out: bfloat16 [8192, 4096], P('ep', 'tp')
Inputs may be any that keep to these rules, and one draw needn't show every extreme that they name: `routes`: each row names 2 different experts. In the rows of one device no expert is named by more than 32 rows, and in the rows of some device an expert is named by exactly 32 rows.
All inputs are finite; a program needn't handle non-finite values.
Results may differ from a plain program's by a relative error of at most 0.0057.
Values may be sent and summed in bfloat16 or wider, within the bound.
No kernel may reach another device: no remote copies, remote signals or barrier semaphores. Data moves between devices by JAX's collectives and lax.ppermute only.
A program may use at most 128 MiB of HBM per device.

v0:
```python
import jax
import jax.numpy as jnp
from jax import lax
from jax.sharding import Mesh
from jax.sharding import PartitionSpec as P

D = 4096
BLOCK = 64
EP = ("ep_0", "ep_1")
EPSILON = 1e-06
LOG_FLOOR = -1e30
HIGHEST_PRECISION = lax.Precision.HIGHEST


def nothing_yet(x, identity):
    return jax.tree.map(
        lambda part, zero: jnp.zeros_like(part) + jnp.asarray(zero, part.dtype), x, identity
    )


def collected_together(x, axis):
    leaves = jax.tree.leaves(x)
    turns = sorted(range(len(leaves)), key=lambda k: -leaves[k].size)
    width = (1, *leaves[turns[0]].shape)[-1]
    lines = [
        jnp.pad(leaves[k].reshape(-1), (0, -leaves[k].size % width)).reshape(-1, width)
        for k in turns
    ]
    both, at, found = (lax.all_gather(jnp.concatenate(lines), axis), 0, {})
    for k, line in zip(turns, lines):
        share = both[:, at : at + len(line)].reshape(len(both), -1)
        found[k] = share[:, : leaves[k].size].reshape(-1, *leaves[k].shape)
        at += len(line)
    numbers = iter(range(len(leaves)))
    return jax.tree.map(lambda _: found[next(numbers)], x)


def prefix_by_axis(x, axes, combine, identity):
    before = start = nothing_yet(x, identity)
    subtotal = x
    for axis in reversed(axes):
        length, index = (lax.axis_size(axis), lax.axis_index(axis))
        pieces = collected_together(subtotal, axis)
        inside, subtotal = (start, start)
        for k in range(length):
            passed = k < index
            subtotal = combine(subtotal, jax.tree.map(lambda part: part[k], pieces))
            inside = jax.tree.map(lambda new, old: jnp.where(passed, new, old), subtotal, inside)
        before = combine(inside, before)
    return before


def joined_along(tiles, dim):
    dims = list(tiles.shape[1:])
    dims[dim] *= tiles.shape[0]
    return jnp.moveaxis(tiles, 0, dim).reshape(dims)


def copy_for_each(x, axis):
    copies = jnp.broadcast_to(x, (lax.axis_size(axis), *x.shape))
    return lax.all_to_all(copies, axis, split_axis=0, concat_axis=0, tiled=True)


def gather_directly(x, axis, dim):
    return joined_along(copy_for_each(x, axis), dim)


def combine(first_part, second_part):
    decay_first, max_first, memory_first, normal_first = first_part
    decay_second, max_second, memory_second, normal_second = second_part
    running_max = jnp.maximum(decay_second + max_first, max_second)
    keep_first = jnp.exp(decay_second + max_first - running_max)
    keep_second = jnp.exp(max_second - running_max)
    memory = (
        keep_first[..., None, None] * memory_first + keep_second[..., None, None] * memory_second
    )
    normalizer = keep_first[..., None] * normal_first + keep_second[..., None] * normal_second
    return (decay_first + decay_second, running_max, memory, normalizer)


def identity_state(head_count, key_width, value_width):
    return (
        jnp.zeros((head_count,), jnp.float32),
        jnp.full((head_count,), LOG_FLOOR, jnp.float32),
        jnp.zeros((head_count, key_width, value_width), jnp.float32),
        jnp.zeros((head_count, key_width), jnp.float32),
    )


def halfprod(form, left, right):
    return jnp.einsum(form, left, right, preferred_element_type=jnp.float32)


def prepare(query_heads, key_heads, value_heads, in_gate, forget_gate):
    head_count, length, key_width = query_heads.shape
    block_count = length // BLOCK
    query_blocks = query_heads.reshape(head_count, block_count, BLOCK, key_width)
    key_blocks = key_heads.reshape(head_count, block_count, BLOCK, key_width)
    value_blocks = value_heads.reshape(head_count, block_count, BLOCK, value_heads.shape[-1])
    log_input = in_gate.reshape(head_count, block_count, BLOCK)
    cumulative = jnp.cumsum(
        jax.nn.log_sigmoid(forget_gate).reshape(head_count, block_count, BLOCK), axis=-1
    )
    block_decay = cumulative[..., -1]
    weight_log = block_decay[..., None] - cumulative + log_input
    block_max = jnp.max(weight_log, axis=-1)
    weighted = (
        key_blocks.astype(jnp.float32) * jnp.exp(weight_log - block_max[..., None])[..., None]
    )
    normalizer = jnp.sum(weighted, axis=2)
    memory = halfprod("hcsk,hcsv->hckv", weighted.astype(jnp.bfloat16), value_blocks)
    return (
        (query_blocks, key_blocks, value_blocks, log_input, cumulative),
        (block_decay, block_max, memory, normalizer),
    )


def prefix(summary, initial):
    leading = jax.tree.map(lambda tensor: jnp.moveaxis(tensor, 1, 0), summary)

    def advance(running, current):
        return (combine(running, current), running)

    final_state, before = lax.scan(advance, initial, leading)
    return (final_state, jax.tree.map(lambda tensor: jnp.moveaxis(tensor, 0, 1), before))


def block_outputs(blocked, before):
    query_blocks, key_blocks, value_blocks, log_input, cumulative = blocked
    prior_max, prior_memory, prior_normal = (before[1], before[2], before[3])
    block_len = cumulative.shape[-1]
    scale = query_blocks.shape[-1] ** (-0.5)
    causal = jnp.tril(jnp.ones((block_len, block_len), dtype=bool))
    log_decay = jnp.where(
        causal,
        cumulative[..., :, None] - cumulative[..., None, :] + log_input[..., None, :],
        -jnp.inf,
    )
    log_inter = cumulative + prior_max[..., None]
    top_value = jnp.maximum(log_inter, jnp.max(log_decay, axis=-1))
    scores = (
        halfprod("hctk,hcsk->hcts", query_blocks, key_blocks)
        * scale
        * jnp.exp(log_decay - top_value[..., None])
    )
    carried = jnp.exp(log_inter - top_value) * scale
    query_wide = query_blocks.astype(jnp.float32)
    numerator = carried[..., None] * jnp.einsum(
        "hctk,hckv->hctv", query_wide, prior_memory, precision=HIGHEST_PRECISION
    ) + halfprod("hcts,hcsv->hctv", scores.astype(jnp.bfloat16), value_blocks)
    denominator = carried * jnp.einsum(
        "hctk,hck->hct", query_wide, prior_normal, precision=HIGHEST_PRECISION
    ) + jnp.sum(scores, axis=-1)
    return numerator / jnp.maximum(jnp.abs(denominator), jnp.exp(-top_value))[..., None]


def finish(head_values, out_gate, head_gain):
    head_count, block_count, block_len, value_width = head_values.shape
    per_head = jnp.transpose(head_values, (1, 2, 0, 3)).reshape(
        block_count * block_len, head_count, value_width
    )
    per_head = per_head * lax.rsqrt(jnp.mean(per_head * per_head, axis=-1, keepdims=True) + EPSILON)
    per_head = per_head.reshape(block_count * block_len, head_count * value_width) * head_gain
    per_head = per_head * jax.nn.sigmoid(out_gate.astype(jnp.float32))
    return per_head.astype(jnp.bfloat16)


def cell_heads(query_rows, key_rows, value_rows, in_gate, forget_gate, out_gate, head_gain):
    length = query_rows.shape[0]
    head_count = in_gate.shape[0]
    key_width = query_rows.shape[1] // head_count
    value_width = value_rows.shape[1] // head_count
    query_heads = query_rows.reshape(length, head_count, key_width).transpose(1, 0, 2)
    key_heads = key_rows.reshape(length, head_count, key_width).transpose(1, 0, 2)
    value_heads = value_rows.reshape(length, head_count, value_width).transpose(1, 0, 2)
    blocked, summary = prepare(query_heads, key_heads, value_heads, in_gate, forget_gate)
    initial = identity_state(head_count, key_width, value_width)
    final_state, before = prefix(summary, initial)
    incoming = prefix_by_axis(final_state, EP, combine, initial)
    expanded = jax.tree.map(lambda tensor: tensor[:, None], incoming)
    before = combine(expanded, before)
    return finish(block_outputs(blocked, before), out_gate, head_gain)


def body(
    query_rows,
    key_rows,
    value_rows,
    in_gate,
    forget_gate,
    out_gate,
    head_gain,
    mix_weight,
    expert_input,
    routes,
    route_weight,
    gate_weight,
    up_weight,
    down_weight,
):
    mixed_heads = cell_heads(
        query_rows, key_rows, value_rows, in_gate, forget_gate, out_gate, head_gain
    )
    gate_local = gate_weight[0]
    up_local = up_weight[0]
    down_local = down_weight[0]
    group_size = lax.axis_size(EP)
    token_count, fanout = routes.shape
    capacity = 2 * token_count * fanout // group_size
    slot_count = group_size * capacity
    chosen = routes.reshape(-1)
    one_hot = (chosen[:, None] == jnp.arange(group_size, dtype=jnp.int32)[None, :]).astype(
        jnp.int32
    )
    position = jnp.sum((jnp.cumsum(one_hot, axis=0) - one_hot) * one_hot, axis=1)
    target = chosen * capacity + position
    matches = (jnp.arange(slot_count, dtype=jnp.int32)[:, None] == target[None, :]).astype(
        jnp.int32
    )
    occupied = jnp.sum(matches, axis=1) > 0
    source_row = jnp.sum(
        matches * (jnp.arange(token_count * fanout, dtype=jnp.int32) // fanout)[None, :], axis=1
    )
    arrived = lax.all_to_all(
        jnp.where(
            occupied[:, None],
            jnp.take(expert_input, source_row, axis=0),
            jnp.zeros((), expert_input.dtype),
        ),
        EP,
        split_axis=0,
        concat_axis=0,
        tiled=True,
    )
    head_piece = lax.all_gather(mixed_heads, "tp", axis=1, tiled=True)
    token_piece = lax.all_gather(arrived, "tp", axis=1, tiled=True)
    mix_acc = jnp.dot(head_piece, mix_weight, preferred_element_type=jnp.float32)
    gate_acc = jnp.einsum("sd,fd->sf", token_piece, gate_local, preferred_element_type=jnp.float32)
    up_acc = jnp.einsum("sd,fd->sf", token_piece, up_local, preferred_element_type=jnp.float32)
    squares = jnp.sum(jnp.square(token_piece.astype(jnp.float32)), axis=1)
    mix_acc, gate_acc, up_acc, squares = (mix_acc, gate_acc, up_acc, squares)
    mixer_out = mix_acc.astype(jnp.bfloat16)
    inverse_rms = lax.rsqrt(squares / D + EPSILON)[:, None]
    hidden = (jax.nn.silu(gate_acc * inverse_rms) * (up_acc * inverse_rms)).astype(jnp.bfloat16)
    expert_rows = jnp.dot(
        gather_directly(hidden, "tp", 1), down_local, preferred_element_type=jnp.float32
    )
    returned_rows = lax.all_to_all(
        expert_rows.astype(jnp.bfloat16), EP, split_axis=0, concat_axis=0, tiled=True
    )
    picked_rows = (
        jnp.take(returned_rows, target, axis=0).reshape(token_count, fanout, -1).astype(jnp.float32)
    )
    expert_out = jnp.sum(picked_rows * route_weight[:, :, None], axis=1).astype(jnp.bfloat16)
    return (mixer_out, expert_out)


def solution(mesh):
    split = Mesh(mesh.devices.reshape(16, 2, mesh.shape["tp"]), ("ep_0", "ep_1", "tp"))
    in_specs = (
        P(EP, "tp"),
        P(EP, "tp"),
        P(EP, "tp"),
        P("tp", EP),
        P("tp", EP),
        P(EP, "tp"),
        P("tp"),
        P(None, "tp"),
        P(EP, "tp"),
        P(EP, None),
        P(EP, None),
        P(EP, "tp", None),
        P(EP, "tp", None),
        P(EP, None, "tp"),
    )
    out_specs = (P(EP, "tp"), P(EP, "tp"))
    return jax.shard_map(body, mesh=split, in_specs=in_specs, out_specs=out_specs, check_vma=False)
```

profile of v0, /device:TPU:1, one launch (start us, length us, event | category | flops | bytes accessed | tf_op | source)
XLA Modules:
  0.0 352.5 jit_solution(5622983685871281707)
XLA Ops:
  7.3 0.8 fusion.55
  8.6 0.5 broadcast.772
  9.1 1.3 reduce.22
  10.6 0.8 reshape.1181
  11.6 1.1 fusion.21
  12.6 1.5 convolution_bitcast_fusion
  14.2 36.5 %while.25 = (s32[]{:T(128)}, f32[1]{0:T(128)}, f32[1]{0:T(128)}, f32[1,128,256]{2,1,0:T(8,128)S(1)}, f32[1,128]{1,0:T(1,128)S(1)}, /*index=5*/f32[8,1]{0,1:T(1,1...) while((s32[]{:T(128)}, f32[1]{0:T(128)}, f32[1]{0:T(128)}, ...), condition=%wide.region_4.5_spmd.clone, body=%wide.region_3.4_spmd.clone.sunk | while | flops 164488 | bytes 659258 | solution.py:124
  14.2 0.6 constant_dynamic-slice_fusion.4
  16.7 0.7 bitcast_dynamic-update-slice_fusion.2
  17.4 0.6 constant_dynamic-update-slice_fusion.2
  18.7 0.6 constant_dynamic-slice_fusion.4
  21.2 0.7 bitcast_dynamic-update-slice_fusion.2
  21.9 0.6 constant_dynamic-update-slice_fusion.2
  23.2 0.6 constant_dynamic-slice_fusion.4
  25.7 0.7 bitcast_dynamic-update-slice_fusion.2
  26.5 0.6 constant_dynamic-update-slice_fusion.2
  27.8 0.6 constant_dynamic-slice_fusion.4
  30.3 0.7 bitcast_dynamic-update-slice_fusion.2
  31.1 0.6 constant_dynamic-update-slice_fusion.2
  32.4 0.6 constant_dynamic-slice_fusion.4
  34.9 0.7 bitcast_dynamic-update-slice_fusion.2
  35.7 0.6 constant_dynamic-update-slice_fusion.2
  37.0 0.6 constant_dynamic-slice_fusion.4
  39.5 0.7 bitcast_dynamic-update-slice_fusion.2
  40.2 0.5 constant_dynamic-update-slice_fusion.2
  41.5 0.6 constant_dynamic-slice_fusion.4
  44.0 0.7 bitcast_dynamic-update-slice_fusion.2
  44.7 0.5 constant_dynamic-update-slice_fusion.2
  46.0 0.6 constant_dynamic-slice_fusion.4
  48.5 0.7 bitcast_dynamic-update-slice_fusion.2
  49.2 0.6 constant_dynamic-update-slice_fusion.2
  50.7 0.5 copy-done.15
  51.2 8.5 %all-gather.2 = f32[2,131,256]{2,1,0:T(8,128)S(1)} all-gather(f32[1,131,256]{2,1,0:T(8,128)S(1)} %maximum_bitcast_fusion), channel_id=2, replica_groups=mesh['ep_0'=16,'ep_1'=2,'tp'=16] {'ep_1'}, dimensions={0}, use_global_device_ids=true | all-gather | bytes 402432 | tf_op jit(solution)/shard_map/all_gather | solution.py:29
  59.7 0.6 fusion.86
  60.3 0.5 fusion.87
  66.3 0.7 maximum_bitcast_fusion.1
  67.0 0.8 copy.54
  68.1 1.2 reduce-window.6
  69.7 0.6 convert_reduce_fusion
  70.5 3.9 %gather_fusion = bf16[1024,256]{1,0:T(8,128)(2,1)S(1)} fusion(bf16[256,256]{1,0:T(8,128)(2,1)S(1)} %copy-done.1, s32[1024]{0:T(1024)S(1)} %broadcast_clamp_fusion), kind=kCustom, calls=%fused_computation | custom fusion | bytes 1052672 | tf_op jit(solution)/shard_map/jit(_take)/gather | solution.py:227
  74.6 0.3 select_select_fusion
  74.9 48.4 %all_to_all.26 = bf16[32,32,256]{2,1,0:T(8,128)(2,1)} all-to-all(bf16[32,32,256]{2,1,0:T(8,128)(2,1)S(1)} %select_select_fusion), channel_id=1, replica_groups=mesh['ep_0'=16,'ep_1'=2,'tp'=16] {'ep_0','ep_1'}, dimensions={0} | all-to-all | bytes 1048576 | tf_op jit(solution)/shard_map/all_to_all | solution.py:224
  124.7 22.1 %all-gather.12.cloned.1.call-done = f32[16,131,256]{2,1,0:T(8,128)} async-done(((f32[1,131,256]{2,1,0:T(8,128)}), f32[16,131,256]{2,1,0:T(8,128)}) %all-gather.12.cloned.1.call-update) | async-done | bytes 2146320 | tf_op jit(solution)/shard_map/all_gather | solution.py:29
  146.8 1.1 fusion.82
  147.9 0.7 fusion.85
  149.2 0.6 fusion.84
  180.3 0.3 fusion.89
  181.0 2.0 fusion.26
  183.0 0.3 fusion.44
  183.3 0.8 multiply_reduce_fusion.2
  184.2 0.9 fusion.17
  185.1 59.3 %all-gather.10.cloned.1.call-done = bf16[1024,4096]{1,0:T(8,128)(2,1)} async-done(((bf16[1024,256]{1,0:T(8,128)(2,1)}), bf16[1024,4096]{1,0:T(8,128)(2,1)}) %all-gather.10.cloned.1.call-update) | async-done | bytes 8388624 | tf_op jit(solution)/shard_map/all_gather | solution.py:236
  244.4 5.2 %multiply_reduce_fusion = f32[1024]{0:T(1024)S(1)} fusion(bf16[1024,4096]{1,0:T(8,128)(2,1)} %all-gather.10.cloned.1.call-done), kind=kLoop, calls=%fused_computation.12 | loop fusion | flops 12581888 | bytes 8392704 | tf_op jit(solution)/shard_map/reduce_sum | solution.py:240
  249.6 0.5 copy-done.2
  250.1 2.7 convolution_multiply_fusion.3
  252.8 2.7 fusion.8
  255.8 35.5 %all_to_all.27 = bf16[16,1024,64]{1,2,0:T(8,128)(2,1)S(1)} all-to-all(bf16[16,1024,64]{1,2,0:T(8,128)(2,1)S(1)} %broadcast_in_dim.75), channel_id=1, replica_groups=mesh['ep_0'=16,'ep_1'=2,'tp'=16] {'tp'}, dimensions={0} | all-to-all | bytes 4194304 | tf_op jit(solution)/shard_map/all_to_all | solution.py:61
  291.3 1.6 convolution_convert_fusion
  292.9 15.3 %all-to-all-start.2 = ((bf16[32,32,256]{2,1,0:T(8,128)(2,1)}), bf16[32,32,256]{2,1,0:T(8,128)(2,1)S(1)}, u32[]{:S(2)}, u32[]{:S(2)}) async-start(bf16[32,32,256]{2,1,0:T(8,128)(2,1)} %bitcast.139), calls=%async_computation.2 | async-start | bytes 1048576 | tf_op jit(solution)/shard_map/all_to_all | solution.py:248
  309.1 22.7 %all-gather.8.cloned.1.call-done = bf16[512,4096]{1,0:T(8,128)(2,1)} async-done(((bf16[512,256]{1,0:T(8,128)(2,1)}), bf16[512,4096]{1,0:T(8,128)(2,1)}) %all-gather.8.cloned.1.call-update) | async-done | bytes 4194320 | tf_op jit(solution)/shard_map/all_gather | solution.py:235
  331.8 4.1 %convolution_convert_fusion.1 = bf16[512,256]{1,0:T(8,128)(2,1)} fusion(bf16[512,4096]{1,0:T(8,128)(2,1)} %all-gather.8.cloned.1.call-done, bf16[4096,256]{1,0:T(8,128)(2,1)S(1)} %copy-done), kind=kOutput, calls=%fused_computation.22 | convolution fusion | flops 1073872896 | bytes 6553600 | tf_op jit(solution)/shard_map/dot_general | solution.py:237
  335.9 5.8 %all-to-all-done.2 = bf16[32,32,256]{2,1,0:T(8,128)(2,1)S(1)} async-done(((bf16[32,32,256]{2,1,0:T(8,128)(2,1)}), bf16[32,32,256]{2,1,0:T(8,128)(2,1)S(1)}, u32[]{:S(2)}, u32[]{:S(2)}) %all-to-all-start.2) | async-done | bytes 524320 | tf_op jit(solution)/shard_map/all_to_all | solution.py:248
  341.7 1.9 gather_fusion.1
  343.8 2.2 multiply_reduce_fusion.1
  (150 shorter events, 6.6 us)
Async XLA Ops:
  7.2 324.6 %copy-start = (bf16[4096,256]{1,0:T(8,128)(2,1)S(1)}, bf16[4096,256]{1,0:T(8,128)(2,1)}, u32[]{:S(2)}) copy-start(bf16[4096,256]{1,0:T(8,128)(2,1)} %param.23) | copy-start | bytes 6291460
  7.2 139.6 %all-gather.12.cloned.1.call-start = ((), (), s32[]{:S(2)}) async-start(), calls=%async_computation.5 | async-start | bytes 2367488 | tf_op jit(solution)/shard_map/all_gather | solution.py:29
  8.4 5.7 %copy-start.7 = (f32[1,8,64]{2,1,0:T(8,128)}, f32[1,8,64]{2,1,0:T(8,128)S(1)}, u32[]{:S(2)}) copy-start(f32[1,8,64]{2,1,0:T(8,128)S(1)} %reduce_window_sum.28) | copy-start | bytes 6148
  11.3 2.8 copy-start.9
  14.1 56.4 %copy-start.1 = (bf16[256,256]{1,0:T(8,128)(2,1)S(1)}, bf16[256,256]{1,0:T(8,128)(2,1)}, u32[]{:S(2)}) copy-start(bf16[256,256]{1,0:T(8,128)(2,1)} %param.24) | copy-start | bytes 393220
  50.6 0.5 copy-start.15
  50.6 0.6 copy-start.17
  67.0 177.4 %all-gather.10.cloned.1.call-start = ((), (), s32[]{:S(2)}) async-start(), calls=%async_computation.4 | async-start | bytes 8912896 | tf_op jit(solution)/shard_map/all_gather | solution.py:236
  74.5 49.9 %copy-start.8 = (f32[1,8,64]{2,1,0:T(8,128)S(1)}, f32[1,8,64]{2,1,0:T(8,128)}, u32[]{:S(2)}) copy-start(f32[1,8,64]{2,1,0:T(8,128)} %copy-done.7) | copy-start | bytes 6148
  74.5 49.9 %copy-start.10 = (f32[8,64]{1,0:T(8,128)S(1)}, f32[8,64]{1,0:T(8,128)}, u32[]{:S(2)}) copy-start(f32[8,64]{1,0:T(8,128)} %copy-done.9) | copy-start | bytes 6148
  74.5 105.5 %copy-start.16 = (f32[8,1]{0,1:T(1,128)S(1)}, f32[8,1]{0,1:T(1,128)}, u32[]{:S(2)}) copy-start(f32[8,1]{0,1:T(1,128)} %copy-done.15) | copy-start | bytes 100
  74.5 105.5 %copy-start.18 = (f32[8,1]{0,1:T(1,128)S(1)}, f32[8,1]{0,1:T(1,128)}, u32[]{:S(2)}) copy-start(f32[8,1]{0,1:T(1,128)} %copy-done.17) | copy-start | bytes 100
  74.5 105.7 %copy-start.12 = (f32[8,1,128]{2,1,0:T(1,128)S(1)}, f32[8,1,128]{2,1,0:T(1,128)}, u32[]{:S(2)}) copy-start(f32[8,1,128]{2,1,0:T(1,128)} %get-tuple-element.83) | copy-start | bytes 12292
  74.5 105.8 %copy-start.22 = (bf16[512,128]{1,0:T(8,128)(2,1)S(1)}, bf16[512,128]{1,0:T(8,128)(2,1)}, u32[]{:S(2)}) copy-start(bf16[512,128]{1,0:T(8,128)(2,1)} %param.16) | copy-start | bytes 393220
  74.5 106.1 %copy-start.5 = (bf16[512,128]{1,0:T(8,128)(2,1)S(1)}, bf16[512,128]{1,0:T(8,128)(2,1)}, u32[]{:S(2)}) copy-start(bf16[512,128]{1,0:T(8,128)(2,1)} %param.17) | copy-start | bytes 393220
  123.3 59.7 %copy-start.3 = (bf16[512,256]{1,0:T(8,128)(2,1)S(1)}, bf16[512,256]{1,0:T(8,128)(2,1)}, u32[]{:S(2)}) copy-start(bf16[512,256]{1,0:T(8,128)(2,1)} %param.18) | copy-start | bytes 786436
  123.3 208.4 %all-gather.8.cloned.1.call-start = ((), (), s32[]{:S(2)}) async-start(), calls=%async_computation.3 | async-start | bytes 4456448 | tf_op jit(solution)/shard_map/all_gather | solution.py:235
  180.3 3.0 copy-start.19
  180.3 3.0 copy-start.23
  183.0 1.2 copy-start.6
  183.0 1.2 copy-start.14
  184.2 65.4 %copy-start.4 = (bf16[1,64,4096]{2,1,0:T(8,128)(2,1)S(1)}, bf16[1,64,4096]{2,1,0:T(8,128)(2,1)}, u32[]{:S(2)}) copy-start(bf16[1,64,4096]{2,1,0:T(8,128)(2,1)} %param.27) | copy-start | bytes 1572868
  244.4 5.8 %copy-start.2 = (bf16[1024,4096]{1,0:T(8,128)(2,1)S(1)}, bf16[1024,4096]{1,0:T(8,128)(2,1)}, u32[]{:S(2)}) copy-start(bf16[1024,4096]{1,0:T(8,128)(2,1)} %all-gather.10.cloned.1.call-done) | copy-start | bytes 25165828
  250.1 2.7 copy-start.20
  255.8 35.5 %copy-start.21 = (bf16[1,1024,256]{2,1,0:T(8,128)(2,1)S(1)}, bf16[1,1024,256]{2,1,0:T(8,128)(2,1)}, u32[]{:S(2)}) copy-start(bf16[1,1024,256]{2,1,0:T(8,128)(2,1)} %param.29) | copy-start | bytes 1572868
  291.3 17.0 %copy-start.11 = (s32[256,2]{0,1:T(2,128)S(1)}, s32[256,2]{0,1:T(2,128)}, u32[]{:S(2)}) copy-start(s32[256,2]{0,1:T(2,128)} %param.25) | copy-start | bytes 6148
  291.3 17.6 %copy-start.13 = (f32[256,2]{0,1:T(2,128)S(1)}, f32[256,2]{0,1:T(2,128)}, u32[]{:S(2)}) copy-start(f32[256,2]{0,1:T(2,128)} %param.26) | copy-start | bytes 6148
  292.9 48.8 %all-to-all-start.2 = ((bf16[32,32,256]{2,1,0:T(8,128)(2,1)}), bf16[32,32,256]{2,1,0:T(8,128)(2,1)S(1)}, u32[]{:S(2)}, u32[]{:S(2)}) async-start(bf16[32,32,256]{2,1,0:T(8,128)(2,1)} %bitcast.139), calls=%async_computation.2 | async-start | bytes 1048576 | tf_op jit(solution)/shard_map/all_to_all | solution.py:248
Sparse Core Ops, SparseCore 0:
  67.1 79.6 all-gather.11
  149.7 94.5 all-gather.9
  247.9 83.7 all-gather.7
where the time goes:
time: 354 us; the launch traced here: 352 us
  waiting for transfers between devices  110 us (31%)
  blocking collectives  92.4 us (26%)
  between operations  51.3 us (14%)
  other arithmetic  28 us (8%)
  local copies, waits for them, and re-layouts  21.5 us (6%)
  loops' own time  19.7 us (6%)
  starting transfers between devices  15.6 us (4%)
  matrix products  14.2 us (4%)
    all_gather x1, waiting for transfers between devices, body(): token_piece = lax.all_gather(arrived, 'tp', axis=1, tiled=True)  59.3 us
    all_to_all x1, blocking collectives, body(): lax.all_to_all(jnp.where(occupied[:, None], jnp.take(expert_input, source...  48.4 us
    all_to_all x1, blocking collectives, copy_for_each(): return lax.all_to_all(copies, axis, split_axis=0, concat_axis=0, tiled=True)  35.5 us
    all_gather x1, waiting for transfers between devices, body(): head_piece = lax.all_gather(mixed_heads, 'tp', axis=1, tiled=True)  22.7 us
    all_gather x1, waiting for transfers between devices, collected_together(): both, at, found = (lax.all_gather(jnp.concatenate(lines), axis), 0, {})  22.1 us
    another operation x1, loops' own time, prefix(): final_state, before = lax.scan(advance, initial, leading)  19.7 us
    all_to_all x1, starting transfers between devices, body(): lax.all_to_all(expert_rows.astype(jnp.bfloat16), EP, split_axis=0, concat...  15.3 us
    dynamic_update_slice x16, other arithmetic, prefix(): final_state, before = lax.scan(advance, initial, leading)  9.85 us
  transfers between devices with their start and end apart: 4, of which 4 were waited for; matrix products, arithmetic and copies ran while one was open for 9% of the time, Pallas kernels for 0%

commit v1 on v0

--- a/solution.py
+++ b/solution.py
@@ -232,7 +232,9 @@
         concat_axis=0,
         tiled=True,
     )
-    head_piece = lax.all_gather(mixed_heads, "tp", axis=1, tiled=True)
+    head_piece = jnp.concatenate(
+        lax.all_to_all(jnp.stack([mixed_heads] * lax.axis_size("tp")), "tp", 0, 0), axis=1
+    )
     token_piece = lax.all_gather(arrived, "tp", axis=1, tiled=True)
     mix_acc = jnp.dot(head_piece, mix_weight, preferred_element_type=jnp.float32)
     gate_acc = jnp.einsum("sd,fd->sf", token_piece, gate_local, preferred_element_type=jnp.float32)

time: 354 us -> 420 us (1.19)
  waiting for transfers between devices: 110 us -> 192 us
  blocking collectives: 92.4 us -> 57.1 us
  starting transfers between devices: 15.6 us -> 27.8 us
  local copies, waits for them, and re-layouts: 21.5 us -> 25.8 us
    all_to_all x0 -> x2, waiting for transfers between devices: none -> 78 us  [the longest x1 55.9 us: body(): lax.all_to_all(jnp.stack([mixed_heads] * lax.axis_size('tp')), 'tp', 0, 0)]
    all_to_all x1 -> x0, blocking collectives: 35.5 us -> none  [copy_for_each(): return lax.all_to_all(copies, axis, split_axis=0, concat_axis=0, tiled=True)]
    all_gather x1 -> x0, waiting for transfers between devices: 22.7 us -> none  [body(): head_piece = lax.all_gather(mixed_heads, 'tp', axis=1, tiled=True)]
    all_to_all x1, waiting for transfers between devices: 5.79 us -> 28.4 us  [body(): lax.all_to_all(expert_rows.astype(jnp.bfloat16), EP, split_axis=0, concat...]
    all_to_all x0 -> x2, starting transfers between devices: none -> 12.3 us  [the longest x1 7.44 us: body(): lax.all_to_all(jnp.stack([mixed_heads] * lax.axis_size('tp')), 'tp', 0, 0)]
  transfers between devices with their start and end apart: 4 -> 5, of which waited for: 4 -> 5; matrix products, arithmetic and copies ran while one was open for 9% -> 6% of each run, Pallas kernels for 0% -> 0%
where the time goes in v1:
time: 420 us; the launch traced here: 419 us
  waiting for transfers between devices  192 us (46%)
  blocking collectives  57.1 us (14%)
  between operations  52 us (12%)
  starting transfers between devices  27.8 us (7%)
  other arithmetic  27.1 us (6%)
  local copies, waits for them, and re-layouts  25.8 us (6%)
  loops' own time  20.9 us (5%)
  matrix products  15.8 us (4%)
    all_gather x1, waiting for transfers between devices, body(): token_piece = lax.all_gather(arrived, 'tp', axis=1, tiled=True)  62.8 us
    all_to_all x1, waiting for transfers between devices, body(): lax.all_to_all(jnp.stack([mixed_heads] * lax.axis_size('tp')), 'tp', 0, 0)  55.9 us
    all_to_all x1, blocking collectives, body(): lax.all_to_all(jnp.where(occupied[:, None], jnp.take(expert_input, source...  48.6 us
    all_to_all x1, waiting for transfers between devices, body(): lax.all_to_all(expert_rows.astype(jnp.bfloat16), EP, split_axis=0, concat...  28.4 us
    all_gather x1, waiting for transfers between devices, collected_together(): both, at, found = (lax.all_gather(jnp.concatenate(lines), axis), 0, {})  22.8 us
    all_to_all x1, waiting for transfers between devices, copy_for_each(): return lax.all_to_all(copies, axis, split_axis=0, concat_axis=0, tiled=True)  22.1 us
    another operation x1, loops' own time, prefix(): final_state, before = lax.scan(advance, initial, leading)  20.9 us
    all_to_all x1, starting transfers between devices, body(): lax.all_to_all(expert_rows.astype(jnp.bfloat16), EP, split_axis=0, concat...  15.4 us
  transfers between devices with their start and end apart: 5, of which 5 were waited for; matrix products, arithmetic and copies ran while one was open for 6% of the time, Pallas kernels for 0%

profile of v1, /device:TPU:1, one launch (start us, length us, event | category | flops | bytes accessed | tf_op | source)
XLA Modules:
  0.0 418.6 jit_solution(3138331151573554497)
XLA Ops:
  7.3 0.8 fusion.55
  8.6 0.5 broadcast.774
  9.1 1.3 reduce.22
  10.6 0.8 reshape.1189
  11.6 1.1 fusion.21
  12.6 1.5 convolution_bitcast_fusion
  14.2 37.9 %while.25 = (s32[]{:T(128)}, f32[1]{0:T(128)}, f32[1]{0:T(128)}, f32[1,128,256]{2,1,0:T(8,128)S(1)}, f32[1,128]{1,0:T(1,128)S(1)}, /*index=5*/f32[8,1]{0,1:T(1,1...) while((s32[]{:T(128)}, f32[1]{0:T(128)}, f32[1]{0:T(128)}, ...), condition=%wide.region_4.5_spmd.clone, body=%wide.region_3.4_spmd.clone.sunk | while | flops 164488 | bytes 659258 | solution.py:124
  14.2 0.6 constant_dynamic-slice_fusion.4
  16.8 0.7 bitcast_dynamic-update-slice_fusion.2
  17.5 0.6 constant_dynamic-update-slice_fusion.2
  18.9 0.6 constant_dynamic-slice_fusion.4
  21.5 0.7 bitcast_dynamic-update-slice_fusion.2
  22.2 0.5 constant_dynamic-update-slice_fusion.2
  23.6 0.7 constant_dynamic-slice_fusion.4
  26.2 0.7 bitcast_dynamic-update-slice_fusion.2
  26.9 0.5 constant_dynamic-update-slice_fusion.2
  28.3 0.7 constant_dynamic-slice_fusion.4
  30.9 0.7 bitcast_dynamic-update-slice_fusion.2
  31.6 0.6 constant_dynamic-update-slice_fusion.2
  33.1 0.7 constant_dynamic-slice_fusion.4
  35.7 0.7 bitcast_dynamic-update-slice_fusion.2
  36.4 0.5 constant_dynamic-update-slice_fusion.2
  37.8 0.7 constant_dynamic-slice_fusion.4
  40.5 0.6 bitcast_dynamic-update-slice_fusion.2
  41.2 0.5 constant_dynamic-update-slice_fusion.2
  42.6 0.7 constant_dynamic-slice_fusion.4
  45.2 0.7 bitcast_dynamic-update-slice_fusion.2
  45.9 0.6 constant_dynamic-update-slice_fusion.2
  47.3 0.7 constant_dynamic-slice_fusion.4
  50.0 0.7 bitcast_dynamic-update-slice_fusion.2
  50.7 0.5 constant_dynamic-update-slice_fusion.2
  52.1 0.5 copy-done.15
  52.6 8.5 %all-gather.2 = f32[2,131,256]{2,1,0:T(8,128)S(1)} all-gather(f32[1,131,256]{2,1,0:T(8,128)S(1)} %maximum_bitcast_fusion), channel_id=2, replica_groups=mesh['ep_0'=16,'ep_1'=2,'tp'=16] {'ep_1'}, dimensions={0}, use_global_device_ids=true | all-gather | bytes 402432 | tf_op jit(solution)/shard_map/all_gather | solution.py:29
  61.1 0.6 fusion.86
  61.7 0.6 fusion.87
  67.5 0.7 maximum_bitcast_fusion.1
  68.3 0.8 copy.58
  69.4 1.2 reduce-window.6
  70.9 0.6 convert_reduce_fusion
  71.8 3.9 gather_fusion
  76.1 48.6 %all_to_all.31 = bf16[32,32,256]{2,1,0:T(8,128)(2,1)} all-to-all(bf16[32,32,256]{2,1,0:T(8,128)(2,1)S(1)} %select_select_fusion), channel_id=1, replica_groups=mesh['ep_0'=16,'ep_1'=2,'tp'=16] {'ep_0','ep_1'}, dimensions={0} | all-to-all | bytes 1048576 | tf_op jit(solution)/shard_map/all_to_all | solution.py:224
  125.9 22.8 %all-gather.9.cloned.1.call-done = f32[16,131,256]{2,1,0:T(8,128)} async-done(((f32[1,131,256]{2,1,0:T(8,128)}), f32[16,131,256]{2,1,0:T(8,128)}) %all-gather.9.cloned.1.call-update) | async-done | bytes 2146320 | tf_op jit(solution)/shard_map/all_gather | solution.py:29
  148.7 1.1 fusion.82
  149.8 0.7 fusion.85
  151.2 0.6 fusion.84
  182.8 62.8 %all-gather.7.cloned.1.call-done = bf16[1024,4096]{1,0:T(8,128)(2,1)} async-done(((bf16[1024,256]{1,0:T(8,128)(2,1)}), bf16[1024,4096]{1,0:T(8,128)(2,1)}) %all-gather.7.cloned.1.call-update) | async-done | bytes 8388624 | tf_op jit(solution)/shard_map/all_gather | solution.py:238
  245.5 5.2 %multiply_reduce_fusion = f32[1024]{0:T(1024)S(1)} fusion(bf16[1024,4096]{1,0:T(8,128)(2,1)} %all-gather.7.cloned.1.call-done), kind=kLoop, calls=%fused_computation.12 | loop fusion | flops 12581888 | bytes 8392704 | tf_op jit(solution)/shard_map/reduce_sum | solution.py:242
  250.8 0.5 copy-done.2
  251.3 2.7 convolution_multiply_fusion.3
  254.0 2.7 fusion.8
  256.7 1.6 broadcast_in_dim.75
  258.3 4.9 %all-to-all-start.2 = ((bf16[16,1024,64]{1,2,0:T(8,128)(2,1)}), bf16[16,1024,64]{1,2,0:T(8,128)(2,1)}, u32[]{:S(2)}, u32[]{:S(2)}) async-start(bf16[16,1024,64]{1,2,0:T(8,128)(2,1)} %broadcast_in_dim.75), calls=%async_computation.2 | async-start | bytes 4194304 | tf_op jit(solution)/shard_map/all_to_all | solution.py:61
  263.9 2.0 fusion.26
  266.2 0.8 multiply_reduce_fusion.2
  267.4 22.1 %all-to-all-done.2 = bf16[16,1024,64]{1,2,0:T(8,128)(2,1)} async-done(((bf16[16,1024,64]{1,2,0:T(8,128)(2,1)}), bf16[16,1024,64]{1,2,0:T(8,128)(2,1)}, u32[]{:S(2)}, u32[]{:S(2)}) %all-to-all-start.2) | async-done | bytes 2097184 | tf_op jit(solution)/shard_map/all_to_all | solution.py:61
  289.6 2.5 stack.2
  292.1 7.4 %all-to-all-start = ((bf16[16,512,256]{1,2,0:T(8,128)(2,1)}), bf16[16,512,256]{1,2,0:T(8,128)(2,1)}, u32[]{:S(2)}, u32[]{:S(2)}) async-start(bf16[16,512,256]{1,2,0:T(8,128)(2,1)} %stack.2), calls=%async_computation | async-start | bytes 8388608 | tf_op jit(solution)/shard_map/all_to_all | solution.py:236
  299.6 3.2 convolution_convert_fusion
  302.7 55.9 %all-to-all-done = bf16[16,512,256]{1,2,0:T(8,128)(2,1)} async-done(((bf16[16,512,256]{1,2,0:T(8,128)(2,1)}), bf16[16,512,256]{1,2,0:T(8,128)(2,1)}, u32[]{:S(2)}, u32[]{:S(2)}) %all-to-all-start) | async-done | bytes 4194336 | tf_op jit(solution)/shard_map/all_to_all | solution.py:236
  358.6 15.4 %all-to-all-start.3 = ((bf16[32,32,256]{2,1,0:T(8,128)(2,1)}), bf16[32,32,256]{2,1,0:T(8,128)(2,1)S(1)}, u32[]{:S(2)}, u32[]{:S(2)}) async-start(bf16[32,32,256]{2,1,0:T(8,128)(2,1)} %bitcast.141), calls=%async_computation.3 | async-start | bytes 1048576 | tf_op jit(solution)/shard_map/all_to_all | solution.py:250
  375.0 4.2 %convolution_convert_fusion.1 = bf16[512,256]{1,0:T(8,128)(2,1)} fusion(bf16[512,4096]{0,1:T(8,128)(2,1)} %bitcast.130, bf16[4096,256]{1,0:T(8,128)(2,1)S(1)} %copy-done), kind=kOutput, calls=%fused_computation.22 | convolution fusion | flops 1073872896 | bytes 6553600 | tf_op jit(solution)/shard_map/dot_general | solution.py:239
  379.1 28.4 %all-to-all-done.3 = bf16[32,32,256]{2,1,0:T(8,128)(2,1)S(1)} async-done(((bf16[32,32,256]{2,1,0:T(8,128)(2,1)}), bf16[32,32,256]{2,1,0:T(8,128)(2,1)S(1)}, u32[]{:S(2)}, u32[]{:S(2)}) %all-to-all-start.3) | async-done | bytes 524320 | tf_op jit(solution)/shard_map/all_to_all | solution.py:250
  407.5 1.9 gather_fusion.1
  409.6 2.2 multiply_reduce_fusion.1
  (150 shorter events, 7.3 us)
Async XLA Ops:
  7.2 367.8 %copy-start = (bf16[4096,256]{1,0:T(8,128)(2,1)S(1)}, bf16[4096,256]{1,0:T(8,128)(2,1)}, u32[]{:S(2)}) copy-start(bf16[4096,256]{1,0:T(8,128)(2,1)} %param.23) | copy-start | bytes 6291460
  7.2 141.5 %all-gather.9.cloned.1.call-start = ((), (), s32[]{:S(2)}) async-start(), calls=%async_computation.5 | async-start | bytes 2367488 | tf_op jit(solution)/shard_map/all_gather | solution.py:29
  8.4 5.7 %copy-start.7 = (f32[1,8,64]{2,1,0:T(8,128)}, f32[1,8,64]{2,1,0:T(8,128)S(1)}, u32[]{:S(2)}) copy-start(f32[1,8,64]{2,1,0:T(8,128)S(1)} %reduce_window_sum.28) | copy-start | bytes 6148
  11.3 2.8 copy-start.9
  14.1 57.6 %copy-start.1 = (bf16[256,256]{1,0:T(8,128)(2,1)S(1)}, bf16[256,256]{1,0:T(8,128)(2,1)}, u32[]{:S(2)}) copy-start(bf16[256,256]{1,0:T(8,128)(2,1)} %param.24) | copy-start | bytes 393220
  52.1 0.5 copy-start.15
  52.1 0.5 copy-start.17
  68.2 177.3 %all-gather.7.cloned.1.call-start = ((), (), s32[]{:S(2)}) async-start(), calls=%async_computation.4 | async-start | bytes 8912896 | tf_op jit(solution)/shard_map/all_gather | solution.py:238
  75.7 49.9 %copy-start.8 = (f32[1,8,64]{2,1,0:T(8,128)S(1)}, f32[1,8,64]{2,1,0:T(8,128)}, u32[]{:S(2)}) copy-start(f32[1,8,64]{2,1,0:T(8,128)} %copy-done.7) | copy-start | bytes 6148
  75.7 49.9 %copy-start.10 = (f32[8,64]{1,0:T(8,128)S(1)}, f32[8,64]{1,0:T(8,128)}, u32[]{:S(2)}) copy-start(f32[8,64]{1,0:T(8,128)} %copy-done.9) | copy-start | bytes 6148
  75.7 106.8 %copy-start.16 = (f32[8,1]{0,1:T(1,128)S(1)}, f32[8,1]{0,1:T(1,128)}, u32[]{:S(2)}) copy-start(f32[8,1]{0,1:T(1,128)} %copy-done.15) | copy-start | bytes 100
  75.8 106.8 %copy-start.18 = (f32[8,1]{0,1:T(1,128)S(1)}, f32[8,1]{0,1:T(1,128)}, u32[]{:S(2)}) copy-start(f32[8,1]{0,1:T(1,128)} %copy-done.17) | copy-start | bytes 100
  149.8 100.9 %copy-start.4 = (bf16[1,64,4096]{2,1,0:T(8,128)(2,1)S(1)}, bf16[1,64,4096]{2,1,0:T(8,128)(2,1)}, u32[]{:S(2)}) copy-start(bf16[1,64,4096]{2,1,0:T(8,128)(2,1)} %param.27) | copy-start | bytes 1572868
  245.5 5.8 %copy-start.2 = (bf16[1024,4096]{1,0:T(8,128)(2,1)S(1)}, bf16[1024,4096]{1,0:T(8,128)(2,1)}, u32[]{:S(2)}) copy-start(bf16[1024,4096]{1,0:T(8,128)(2,1)} %all-gather.7.cloned.1.call-done) | copy-start | bytes 25165828
  251.3 2.7 copy-start.20
  258.3 4.9 %copy-start.12 = (f32[8,1,128]{2,1,0:T(1,128)S(1)}, f32[8,1,128]{2,1,0:T(1,128)}, u32[]{:S(2)}) copy-start(f32[8,1,128]{2,1,0:T(1,128)} %get-tuple-element.83) | copy-start | bytes 12292
  258.3 5.0 %copy-start.22 = (bf16[512,128]{1,0:T(8,128)(2,1)S(1)}, bf16[512,128]{1,0:T(8,128)(2,1)}, u32[]{:S(2)}) copy-start(bf16[512,128]{1,0:T(8,128)(2,1)} %param.16) | copy-start | bytes 393220
  258.3 5.3 %copy-start.5 = (bf16[512,128]{1,0:T(8,128)(2,1)S(1)}, bf16[512,128]{1,0:T(8,128)(2,1)}, u32[]{:S(2)}) copy-start(bf16[512,128]{1,0:T(8,128)(2,1)} %param.17) | copy-start | bytes 393220
  258.3 31.3 %all-to-all-start.2 = ((bf16[16,1024,64]{1,2,0:T(8,128)(2,1)}), bf16[16,1024,64]{1,2,0:T(8,128)(2,1)}, u32[]{:S(2)}, u32[]{:S(2)}) async-start(bf16[16,1024,64]{1,2,0:T(8,128)(2,1)} %broadcast_in_dim.75), calls=%async_computation.2 | async-start | bytes 4194304 | tf_op jit(solution)/shard_map/all_to_all | solution.py:61
  263.1 2.8 copy-start.3
  263.2 3.0 copy-start.19
  265.9 1.2 copy-start.6
  265.9 1.2 copy-start.14
  292.1 7.5 %copy-start.21 = (bf16[1,1024,256]{2,1,0:T(8,128)(2,1)S(1)}, bf16[1,1024,256]{2,1,0:T(8,128)(2,1)}, u32[]{:S(2)}) copy-start(bf16[1,1024,256]{2,1,0:T(8,128)(2,1)} %param.29) | copy-start | bytes 1572868
  292.1 66.5 %all-to-all-start = ((bf16[16,512,256]{1,2,0:T(8,128)(2,1)}), bf16[16,512,256]{1,2,0:T(8,128)(2,1)}, u32[]{:S(2)}, u32[]{:S(2)}) async-start(bf16[16,512,256]{1,2,0:T(8,128)(2,1)} %stack.2), calls=%async_computation | async-start | bytes 8388608 | tf_op jit(solution)/shard_map/all_to_all | solution.py:236
  299.5 74.6 %copy-start.11 = (s32[256,2]{0,1:T(2,128)S(1)}, s32[256,2]{0,1:T(2,128)}, u32[]{:S(2)}) copy-start(s32[256,2]{0,1:T(2,128)} %param.25) | copy-start | bytes 6148
  299.5 75.2 %copy-start.13 = (f32[256,2]{0,1:T(2,128)S(1)}, f32[256,2]{0,1:T(2,128)}, u32[]{:S(2)}) copy-start(f32[256,2]{0,1:T(2,128)} %param.26) | copy-start | bytes 6148
  358.6 49.0 %all-to-all-start.3 = ((bf16[32,32,256]{2,1,0:T(8,128)(2,1)}), bf16[32,32,256]{2,1,0:T(8,128)(2,1)S(1)}, u32[]{:S(2)}, u32[]{:S(2)}) async-start(bf16[32,32,256]{2,1,0:T(8,128)(2,1)} %bitcast.141), calls=%async_computation.3 | async-start | bytes 1048576 | tf_op jit(solution)/shard_map/all_to_all | solution.py:250
Sparse Core Ops, SparseCore 0:
  68.3 80.3 all-gather.8
  151.7 93.8 all-gather.6
